TPU v7x, 128 devices: a whole 4x4x4 slice. The times are simulated.
128 devices in a mesh: sp: 16 (over z, y), tp: 8 (over x, core).
Axes of the slice: x: 4, y: 4, z: 4, core: 2. Of those that a mesh axis runs over, the one named last changes fastest.
Arguments:
- hidden: bfloat16 [6144, 4096], P('sp', 'tp'), may hold values from -6 to 6
- doc_ids: int32 [6144], P('sp'), may hold values from 0 to 7, never falling along the last dimension, each value on 1 to 1536 neighbouring positions
- norm_gain: float32 [3, 4096], replicated, may hold values from 0.1 to 1.9
- w_value: bfloat16 [3, 4096, 2048], P(None, 'sp', 'tp'), may hold values from -0.09375 to 0.09375
- w_gate: bfloat16 [3, 4096, 2048], P(None, 'sp', 'tp'), may hold values from -0.09375 to 0.09375
- conv_taps: float32 [3, 31, 2048], P(None, None, 'tp'), may hold values from -1 to 1
- conv_bias: float32 [3, 2048], P(None, 'tp'), may hold values from -3 to 3
- chan_gain: float32 [3, 2048], P(None, 'tp'), may hold values from 0.1 to 1.9
- chan_bias: float32 [3, 2048], P(None, 'tp'), may hold values from -3 to 3
- w_out: bfloat16 [3, 2048, 4096], P(None, 'sp', 'tp'), may hold values from -0.125 to 0.125
Outputs:
- result: bfloat16 [6144, 4096], P('sp', 'tp')
Inputs may be any that keep to these rules, and one draw needn't show every extreme that they name: `doc_ids`: document numbers never fall along the sequence; each document has 1 to 1536 positions and one has exactly that many.
All inputs are finite; a program needn't handle non-finite values.
Results may differ from a plain program's by a relative error of at most 0.013.
Values may be sent and summed in bfloat16 or wider, within the bound.
No kernel may reach another device: no remote copies, remote signals or barrier semaphores. Data moves between devices by JAX's collectives and lax.ppermute only.
A program may use at most 128 MiB of HBM per device.

v0:
```python
import jax
import jax.numpy as jnp
from jax import lax
from jax.sharding import PartitionSpec as P

LAYERS = 3


def side_by_side(arrays, axis, dim, along):
    ends, at = ([], 0)
    for a in arrays[:-1]:
        at += a.shape[along]
        ends.append(at)
    both = jnp.concatenate(arrays, axis=along)
    return tuple(jnp.split(lax.all_gather(both, axis, axis=dim, tiled=True), ends, axis=along))


def from_behind(shard, axis, by):
    size = lax.axis_size(axis)
    pairs = [(i, i + by) for i in range(size) if 0 <= i + by < size]
    return lax.ppermute(shard, axis, pairs)


def sent_to_all(shard, axis):
    size = lax.axis_size(axis)
    return lax.all_to_all(
        jnp.broadcast_to(shard[None], (size, *shard.shape)), axis, 0, 0, tiled=True
    )


def of_everyone(shard, axis):
    return sent_to_all(shard, axis).sum(axis=0)


def in_one(arrays, axis):
    ends = [0]
    for a in arrays:
        ends.append(ends[-1] + a.size)
    total = of_everyone(jnp.concatenate([a.ravel() for a in arrays]), axis)
    return tuple((total[b:e].reshape(a.shape) for a, b, e in zip(arrays, ends, ends[1:])))


def joined_along(blocks, dim):
    blocks = jnp.moveaxis(blocks, 0, dim)
    shape = blocks.shape
    return blocks.reshape(*shape[:dim], shape[dim] * shape[dim + 1], *shape[dim + 2 :])


def gather_directly(shard, axis, dim):
    return joined_along(sent_to_all(shard, axis), dim)


def per_device(
    hidden, doc_ids, norm_gain, w_value, w_gate, conv_taps, conv_bias, chan_gain, chan_bias, w_out
):
    width = conv_taps.shape[1]
    length = hidden.shape[0]
    chan_local = w_value.shape[2]
    chan_total = chan_local * lax.axis_size("tp")
    seg_own = doc_ids + 1
    value_all, gate_all, out_all = (
        *side_by_side((w_value, w_gate), "sp", 1, 0),
        lax.all_gather(w_out, "sp", axis=1, tiled=True),
    )
    state = hidden
    for layer in range(LAYERS):
        whole = lax.all_gather(state, "tp", axis=1, tiled=True)
        xwhole = whole.astype(jnp.float32)
        scale = lax.rsqrt(jnp.mean(xwhole * xwhole, axis=-1, keepdims=True) + 1e-06)
        normed = (xwhole * scale * norm_gain[layer]).astype(jnp.bfloat16)
        value = jnp.dot(normed, value_all[layer], preferred_element_type=jnp.float32)
        gate = jnp.dot(normed, gate_all[layer], preferred_element_type=jnp.float32)
        glu = (value * jax.nn.sigmoid(gate)).astype(jnp.bfloat16)
        halo_glu, halo_seg = from_behind(
            (glu[length - (width - 1) :], seg_own[length - (width - 1) :]), "sp", 1
        )
        extended = jnp.concatenate([halo_glu, glu], axis=0).astype(jnp.float32)
        seg_ext = jnp.concatenate([halo_seg.astype(jnp.int32), seg_own], axis=0)
        taps = conv_taps[layer]
        conv = jnp.zeros((length, chan_local), jnp.float32) + conv_bias[layer]
        for index in range(width):
            keep = (seg_ext[index : index + length] == seg_own)[:, None]
            conv = conv + jnp.where(keep, extended[index : index + length] * taps[index], 0.0)
        total, square = in_one((jnp.sum(conv, axis=-1), jnp.sum(conv * conv, axis=-1)), "tp")
        mean_val = (total / chan_total)[:, None]
        var_val = (square / chan_total)[:, None] - mean_val * mean_val
        mixed = jax.nn.silu(
            (conv - mean_val) * lax.rsqrt(var_val + 1e-05) * chan_gain[layer] + chan_bias[layer]
        ).astype(jnp.bfloat16)
        mixed_all = gather_directly(mixed, "tp", 1)
        branch = jnp.dot(mixed_all, out_all[layer], preferred_element_type=jnp.float32)
        state = (state.astype(jnp.float32) + branch).astype(jnp.bfloat16)
    return state


def solution(mesh):
    placed = (
        P("sp", "tp"),
        P("sp"),
        P(),
        P(None, "sp", "tp"),
        P(None, "sp", "tp"),
        P(None, None, "tp"),
        P(None, "tp"),
        P(None, "tp"),
        P(None, "tp"),
        P(None, "sp", "tp"),
    )
    return jax.shard_map(
        per_device, mesh=mesh, in_specs=placed, out_specs=P("sp", "tp"), check_vma=False
    )
```

profile of v0, /device:TPU:32, one launch (start us, length us, event | category | flops | bytes accessed | tf_op | source)
XLA Modules:
  0.0 367.8 jit_solution(13401062077988971587)
XLA Ops:
  10.3 3.5 collective-permute-start
  13.9 3.9 %collective-permute-done = s32[30]{0:T(128)S(1)} collective-permute-done((s32[30]{0:T(128)S(1)}, s32[30]{0:T(128)S(1)}, u32[]{:S(2)}, u32[]{:S(2)}) %collective-permute-start) | collective-permute-done | bytes 152 | tf_op jit(solution)/shard_map/ppermute | solution.py:21
  18.0 20.7 %all-gather.6.cloned.1.call-done = bf16[384,4096]{1,0:T(8,128)(2,1)} async-done(((bf16[384,512]{1,0:T(8,128)(2,1)}), bf16[384,4096]{1,0:T(8,128)(2,1)}) %all-gather.6.cloned.1.call-update) | async-done | bytes 3145744 | tf_op jit(solution)/shard_map/all_gather | solution.py:67
  38.8 2.7 fusion
  41.5 89.1 %all-gather.8.cloned.1.call-done = bf16[6,4096,256]{2,1,0:T(8,128)(2,1)} async-done(((bf16[6,256,256]{2,1,0:T(8,128)(2,1)}), bf16[6,4096,256]{2,1,0:T(8,128)(2,1)}) %all-gather.8.cloned.1.call-update) | async-done | bytes 12582928 | tf_op jit(solution)/shard_map/all_gather | solution.py:15
  138.2 5.4 %collective-permute-done.1 = bf16[30,256]{1,0:T(8,128)(2,1)S(1)} collective-permute-done((bf16[30,256]{1,0:T(8,128)(2,1)S(1)}, bf16[30,256]{1,0:T(8,128)(2,1)S(1)}, u32[]{:S(2)}, u32[]{:S(2)}) %collective-permute-start.1) | collective-permute-done | bytes 15392 | tf_op jit(solution)/shard_map/ppermute | solution.py:21
  143.7 3.4 fusion.233
  147.8 4.3 %all-to-all-start = ((f32[8,1,768]{2,1,0:T(1,128)}), f32[8,1,768]{2,1,0:T(1,128)S(1)}, u32[]{:S(2)}, u32[]{:S(2)}) async-start(f32[8,1,768]{2,1,0:T(1,128)} %broadcast_in_dim.604), calls=%async_computation | async-start | bytes 49152 | tf_op jit(solution)/shard_map/all_to_all | solution.py:26
  152.0 5.4 %all-to-all-done = f32[8,1,768]{2,1,0:T(1,128)S(1)} async-done(((f32[8,1,768]{2,1,0:T(1,128)}), f32[8,1,768]{2,1,0:T(1,128)S(1)}, u32[]{:S(2)}, u32[]{:S(2)}) %all-to-all-start) | async-done | bytes 24608 | tf_op jit(solution)/shard_map/all_to_all | solution.py:26
  159.2 3.6 all-to-all-start.1
  162.8 31.0 %all-gather.10.cloned.1.call-done = bf16[3,2048,512]{2,1,0:T(8,128)(2,1)} async-done(((bf16[3,128,512]{2,1,0:T(8,128)(2,1)}), bf16[3,2048,512]{2,1,0:T(8,128)(2,1)}) %all-gather.10.cloned.1.call-update) | async-done | bytes 6291472 | tf_op jit(solution)/shard_map/all_gather | solution.py:63
  193.8 3.3 fusion.23
  197.2 27.5 %all-gather.12.cloned.1.call-done = bf16[384,4096]{1,0:T(8,128)(2,1)} async-done(((bf16[384,512]{1,0:T(8,128)(2,1)}), bf16[384,4096]{1,0:T(8,128)(2,1)}) %all-gather.12.cloned.1.call-update) | async-done | bytes 3145744 | tf_op jit(solution)/shard_map/all_gather | solution.py:67
  224.7 2.7 fusion.3
  227.6 2.7 fusion.36
  230.2 2.7 fusion.40
  232.9 3.4 collective-permute-start.2
  236.4 4.3 %collective-permute-done.2 = bf16[30,256]{1,0:T(8,128)(2,1)S(1)} collective-permute-done((bf16[30,256]{1,0:T(8,128)(2,1)S(1)}, bf16[30,256]{1,0:T(8,128)(2,1)S(1)}, u32[]{:S(2)}, u32[]{:S(2)}) %collective-permute-start.2) | collective-permute-done | bytes 15392 | tf_op jit(solution)/shard_map/ppermute | solution.py:21
  240.7 3.4 fusion.232
  244.2 8.3 %all_to_all.33 = f32[8,1,768]{2,1,0:T(1,128)S(1)} all-to-all(f32[8,1,768]{2,1,0:T(1,128)S(1)} %broadcast_in_dim.606), channel_id=1, replica_groups=mesh['sp'=16,'tp'=8] {'tp'}, dimensions={0} | all-to-all | bytes 49152 | tf_op jit(solution)/shard_map/all_to_all | solution.py:26
  253.1 24.0 %all_to_all.34 = bf16[8,384,256]{1,2,0:T(8,128)(2,1)S(1)} all-to-all(bf16[8,384,256]{1,2,0:T(8,128)(2,1)S(1)} %broadcast_in_dim.607), channel_id=1, replica_groups=mesh['sp'=16,'tp'=8] {'tp'}, dimensions={0} | all-to-all | bytes 3145728 | tf_op jit(solution)/shard_map/all_to_all | solution.py:26
  277.1 3.4 fusion.22
  280.5 25.1 %all-gather.14.cloned.1.call-done = bf16[384,4096]{1,0:T(8,128)(2,1)} async-done(((bf16[384,512]{1,0:T(8,128)(2,1)}), bf16[384,4096]{1,0:T(8,128)(2,1)}) %all-gather.14.cloned.1.call-update) | async-done | bytes 3145744 | tf_op jit(solution)/shard_map/all_gather | solution.py:67
  305.6 2.7 fusion.6
  308.4 2.7 fusion.34
  311.1 2.7 fusion.39
  313.8 3.4 collective-permute-start.3
  317.2 4.3 %collective-permute-done.3 = bf16[30,256]{1,0:T(8,128)(2,1)S(1)} collective-permute-done((bf16[30,256]{1,0:T(8,128)(2,1)S(1)}, bf16[30,256]{1,0:T(8,128)(2,1)S(1)}, u32[]{:S(2)}, u32[]{:S(2)}) %collective-permute-start.3) | collective-permute-done | bytes 15392 | tf_op jit(solution)/shard_map/ppermute | solution.py:21
  321.6 3.4 fusion.231
  325.1 8.3 %all_to_all.35 = f32[8,1,768]{2,1,0:T(1,128)S(1)} all-to-all(f32[8,1,768]{2,1,0:T(1,128)S(1)} %broadcast_in_dim.608), channel_id=1, replica_groups=mesh['sp'=16,'tp'=8] {'tp'}, dimensions={0} | all-to-all | bytes 49152 | tf_op jit(solution)/shard_map/all_to_all | solution.py:26
  333.9 24.0 %all_to_all.36 = bf16[8,384,256]{1,2,0:T(8,128)(2,1)S(1)} all-to-all(bf16[8,384,256]{1,2,0:T(8,128)(2,1)S(1)} %broadcast_in_dim.609), channel_id=1, replica_groups=mesh['sp'=16,'tp'=8] {'tp'}, dimensions={0} | all-to-all | bytes 3145728 | tf_op jit(solution)/shard_map/all_to_all | solution.py:26
  358.0 3.4 fusion.21
  (83 shorter events, 15.6 us)
Async XLA Ops:
  6.5 3.7 copy-start.8
  6.5 7.2 %copy-start.9 = (f32[3,256]{1,0:T(4,128)S(1)}, f32[3,256]{1,0:T(4,128)}, u32[]{:S(2)}) copy-start(f32[3,256]{1,0:T(4,128)} %param.16) | copy-start | bytes 9220
  6.5 7.3 %copy-start.6 = (f32[3,31,256]{2,1,0:T(8,128)S(1)}, f32[3,31,256]{2,1,0:T(8,128)}, u32[]{:S(2)}) copy-start(f32[3,31,256]{2,1,0:T(8,128)} %param.15) | copy-start | bytes 285700
  6.5 7.3 %copy-start.7 = (f32[3,4096]{1,0:T(4,128)S(1)}, f32[3,4096]{1,0:T(4,128)}, u32[]{:S(2)}) copy-start(f32[3,4096]{1,0:T(4,128)} %param.12) | copy-start | bytes 147460
  6.5 7.4 %copy-start.10 = (f32[3,256]{1,0:T(4,128)S(1)}, f32[3,256]{1,0:T(4,128)}, u32[]{:S(2)}) copy-start(f32[3,256]{1,0:T(4,128)} %param.17) | copy-start | bytes 9220
  6.5 32.2 %all-gather.6.cloned.1.call-start = ((), (), s32[]{:S(2)}) async-start(), calls=%async_computation.6 | async-start | bytes 3538944 | tf_op jit(solution)/shard_map/all_gather | solution.py:67
  7.3 123.3 %all-gather.8.cloned.1.call-start = ((), (), s32[]{:S(2)}) async-start(), calls=%async_computation.7 | async-start | bytes 13369344 | tf_op jit(solution)/shard_map/all_gather | solution.py:15
  9.5 184.3 %all-gather.10.cloned.1.call-start = ((), (), s32[]{:S(2)}) async-start(), calls=%async_computation.8 | async-start | bytes 6684672 | tf_op jit(solution)/shard_map/all_gather | solution.py:63
  10.3 7.6 %collective-permute-start = (s32[30]{0:T(128)S(1)}, s32[30]{0:T(128)S(1)}, u32[]{:S(2)}, u32[]{:S(2)}) collective-permute-start(s32[30]{0:T(128)S(1)} %slice.999), channel_id=1, source_target_pairs={{0,8},{8,16},{16,24},{24,32},{32,40},{40,48},{48,56},{56,64},{64,7... | collective-permute-start | bytes 368 | tf_op jit(solution)/shard_map/ppermute | solution.py:21
  38.8 91.8 %copy-start = (bf16[384,4096]{1,0:T(8,128)(2,1)S(1)}, bf16[384,4096]{1,0:T(8,128)(2,1)}, u32[]{:S(2)}) copy-start(bf16[384,4096]{1,0:T(8,128)(2,1)} %all-gather.6.cloned.1.call-done) | copy-start | bytes 9437188
  135.9 7.7 %collective-permute-start.1 = (bf16[30,256]{1,0:T(8,128)(2,1)S(1)}, bf16[30,256]{1,0:T(8,128)(2,1)S(1)}, u32[]{:S(2)}, u32[]{:S(2)}) collective-permute-start(bf16[30,256]{1,0:T(8,128)(2,1)S(1)} %slice.1247), channel_id=1, source_target_pairs={{0,8},{8,16},{16,24},{24,32},{32,40},{40,48},{48,56},{56,64},{64,7... | collective-permute-start | bytes 46088 | tf_op jit(solution)/shard_map/ppermute | solution.py:21
  143.7 8.3 %copy-start.11 = (f32[3,256]{1,0:T(4,128)S(1)}, f32[3,256]{1,0:T(4,128)}, u32[]{:S(2)}) copy-start(f32[3,256]{1,0:T(4,128)} %param.18) | copy-start | bytes 9220
  147.1 46.7 %copy-start.3 = (bf16[384,512]{1,0:T(8,128)(2,1)S(1)}, bf16[384,512]{1,0:T(8,128)(2,1)}, u32[]{:S(2)}) copy-start(bf16[384,512]{1,0:T(8,128)(2,1)} %param.10) | copy-start | bytes 1179652
  147.8 9.7 %all-to-all-start = ((f32[8,1,768]{2,1,0:T(1,128)}), f32[8,1,768]{2,1,0:T(1,128)S(1)}, u32[]{:S(2)}, u32[]{:S(2)}) async-start(f32[8,1,768]{2,1,0:T(1,128)} %broadcast_in_dim.604), calls=%async_computation | async-start | bytes 49152 | tf_op jit(solution)/shard_map/all_to_all | solution.py:26
  159.2 34.6 %all-to-all-start.1 = ((bf16[8,384,256]{1,2,0:T(8,128)(2,1)}), bf16[8,384,256]{1,2,0:T(8,128)(2,1)S(1)}, u32[]{:S(2)}, u32[]{:S(2)}) async-start(bf16[8,384,256]{1,2,0:T(8,128)(2,1)} %broadcast_in_dim.605), calls=%async_computation.1 | async-start | bytes 3145728 | tf_op jit(solution)/shard_map/all_to_all | solution.py:26
  162.8 62.0 %all-gather.12.cloned.1.call-start = ((), (), s32[]{:S(2)}) async-start(), calls=%async_computation.9 | async-start | bytes 3538944 | tf_op jit(solution)/shard_map/all_gather | solution.py:67
  197.1 108.5 %all-gather.14.cloned.1.call-start = ((), (), s32[]{:S(2)}) async-start(), calls=%async_computation.10 | async-start | bytes 3538944 | tf_op jit(solution)/shard_map/all_gather | solution.py:67
  224.7 2.8 copy-start.1
  232.9 7.7 %collective-permute-start.2 = (bf16[30,256]{1,0:T(8,128)(2,1)S(1)}, bf16[30,256]{1,0:T(8,128)(2,1)S(1)}, u32[]{:S(2)}, u32[]{:S(2)}) collective-permute-start(bf16[30,256]{1,0:T(8,128)(2,1)S(1)} %slice.1282), channel_id=1, source_target_pairs={{0,8},{8,16},{16,24},{24,32},{32,40},{40,48},{48,56},{56,64},{64,7... | collective-permute-start | bytes 46088 | tf_op jit(solution)/shard_map/ppermute | solution.py:21
  244.1 33.0 %copy-start.5 = (bf16[384,512]{1,0:T(8,128)(2,1)S(1)}, bf16[384,512]{1,0:T(8,128)(2,1)}, u32[]{:S(2)}) copy-start(bf16[384,512]{1,0:T(8,128)(2,1)} %fusion.23) | copy-start | bytes 1179652
  305.6 2.8 copy-start.2
  313.8 7.7 %collective-permute-start.3 = (bf16[30,256]{1,0:T(8,128)(2,1)S(1)}, bf16[30,256]{1,0:T(8,128)(2,1)S(1)}, u32[]{:S(2)}, u32[]{:S(2)}) collective-permute-start(bf16[30,256]{1,0:T(8,128)(2,1)S(1)} %slice.1317), channel_id=1, source_target_pairs={{0,8},{8,16},{16,24},{24,32},{32,40},{40,48},{48,56},{56,64},{64,7... | collective-permute-start | bytes 46088 | tf_op jit(solution)/shard_map/ppermute | solution.py:21
  325.0 32.9 %copy-start.4 = (bf16[384,512]{1,0:T(8,128)(2,1)S(1)}, bf16[384,512]{1,0:T(8,128)(2,1)}, u32[]{:S(2)}) copy-start(bf16[384,512]{1,0:T(8,128)(2,1)} %fusion.22) | copy-start | bytes 1179652
Sparse Core Ops, SparseCore 0:
  9.0 29.6 all-gather.5
  40.9 89.6 all-gather.7
  132.7 60.9 all-gather.9
  197.2 27.4 all-gather.11
  280.6 24.9 all-gather.13
where the time goes:
time: 369 us; the launch traced here: 368 us
  waiting for transfers between devices  218 us (59%)
  blocking collectives  64.6 us (18%)
  matrix products  26 us (7%)
  other arithmetic  21.8 us (6%)
  starting transfers between devices  20.5 us (6%)
  between operations  13.6 us (4%)
    all_gather x1, waiting for transfers between devices, side_by_side(): lax.all_gather(both, axis, axis=dim, tiled=True)  89.1 us
    all_gather x3, waiting for transfers between devices, per_device(): whole = lax.all_gather(state, 'tp', axis=1, tiled=True)  73.4 us
    all_to_all x4, blocking collectives, sent_to_all(): lax.all_to_all(jnp.broadcast_to(shard[None], (size, *shard.shape)), axis,...  64.6 us
    all_gather x1, waiting for transfers between devices, per_device(): lax.all_gather(w_out, 'sp', axis=1, tiled=True)  31 us
    ppermute x4, waiting for transfers between devices, from_behind(): return lax.ppermute(shard, axis, pairs)  18 us
    ppermute x4, starting transfers between devices, from_behind(): return lax.ppermute(shard, axis, pairs)  12.5 us
    reduce_sum x3, other arithmetic, per_device(): jnp.sum(conv, axis=-1)  10.2 us
    dot_general x3, matrix products, per_device(): jnp.dot(mixed_all, out_all[layer], preferred_element_type=jnp.float32)  10 us
  transfers between devices with their start and end apart: 11, of which 10 were waited for; matrix products, arithmetic and copies ran while one was open for 4% of the time, Pallas kernels for 0%

commit v1 on v0

--- a/solution.py
+++ b/solution.py
@@ -64,7 +64,7 @@
     )
     state = hidden
     for layer in range(LAYERS):
-        whole = lax.all_gather(state, "tp", axis=1, tiled=True)
+        whole = jnp.concatenate(lax.all_gather(state, "tp"), axis=1)
         xwhole = whole.astype(jnp.float32)
         scale = lax.rsqrt(jnp.mean(xwhole * xwhole, axis=-1, keepdims=True) + 1e-06)
         normed = (xwhole * scale * norm_gain[layer]).astype(jnp.bfloat16)

time: 369 us -> 382 us (1.035)
  local copies, waits for them, and re-layouts: 3.2 us -> 18.9 us
  waiting for transfers between devices: 218 us -> 211 us
    convert_element_type x0 -> x3, local copies, waits for them, and re-layouts: none -> 13.9 us  [the longest x2 11.1 us: per_device(): xwhole = whole.astype(jnp.float32)]
    convert_element_type x0 -> x3, other arithmetic: none -> 7.46 us  [per_device(): normed = (xwhole * scale * norm_gain[layer]).astype(jnp.bfloat16)]
    reduce_sum x3, other arithmetic: 8.2 us -> 4.12 us  [per_device(): scale = lax.rsqrt(jnp.mean(xwhole * xwhole, axis=-1, keepdims=True) + 1e-06)]
    all_gather x1, waiting for transfers between devices: 89.1 us -> 85.2 us  [side_by_side(): lax.all_gather(both, axis, axis=dim, tiled=True)]
  transfers between devices with their start and end apart: 11 -> 11, of which waited for: 10 -> 10; matrix products, arithmetic and copies ran while one was open for 4% -> 6% of each run, Pallas kernels for 0% -> 0%
where the time goes in v1:
time: 382 us; the launch traced here: 381 us
  waiting for transfers between devices  211 us (55%)
  blocking collectives  64.6 us (17%)
  matrix products  27 us (7%)
  other arithmetic  25.1 us (7%)
  starting transfers between devices  20.7 us (5%)
  local copies, waits for them, and re-layouts  18.9 us (5%)
  between operations  13.7 us (4%)
    all_gather x1, waiting for transfers between devices, side_by_side(): lax.all_gather(both, axis, axis=dim, tiled=True)  85.2 us
    all_gather x3, waiting for transfers between devices, per_device(): whole = jnp.concatenate(lax.all_gather(state, 'tp'), axis=1)  73.3 us
    all_to_all x4, blocking collectives, sent_to_all(): lax.all_to_all(jnp.broadcast_to(shard[None], (size, *shard.shape)), axis,...  64.6 us
    all_gather x1, waiting for transfers between devices, per_device(): lax.all_gather(w_out, 'sp', axis=1, tiled=True)  29.7 us
    ppermute x4, waiting for transfers between devices, from_behind(): return lax.ppermute(shard, axis, pairs)  16.1 us
    ppermute x4, starting transfers between devices, from_behind(): return lax.ppermute(shard, axis, pairs)  12.7 us
    convert_element_type x2, local copies, waits for them, and re-layouts, per_device(): xwhole = whole.astype(jnp.float32)  11.1 us
    reduce_sum x3, other arithmetic, per_device(): jnp.sum(conv, axis=-1)  10.2 us
  transfers between devices with their start and end apart: 11, of which 10 were waited for; matrix products, arithmetic and copies ran while one was open for 6% of the time, Pallas kernels for 0%

profile of v1, /device:TPU:32, one launch (start us, length us, event | category | flops | bytes accessed | tf_op | source)
XLA Modules:
  0.0 381.3 jit_solution(2066537456518714855)
XLA Ops:
  10.3 3.5 collective-permute-start
  18.0 20.7 %all-gather.13.cloned.1.call-done = bf16[3072,512]{1,0:T(8,128)(2,1)} async-done(((bf16[384,512]{1,0:T(8,128)(2,1)}), bf16[3072,512]{1,0:T(8,128)(2,1)}) %all-gather.13.cloned.1.call-update) | async-done | bytes 3145744 | tf_op jit(solution)/shard_map/all_gather | solution.py:67
  38.7 2.7 fusion
  42.5 2.8 copy.28
  45.4 85.2 %all-gather.9.cloned.1.call-done = bf16[6,4096,256]{2,1,0:T(8,128)(2,1)} async-done(((bf16[6,256,256]{2,1,0:T(8,128)(2,1)}), bf16[6,4096,256]{2,1,0:T(8,128)(2,1)}) %all-gather.9.cloned.1.call-update) | async-done | bytes 12582928 | tf_op jit(solution)/shard_map/all_gather | solution.py:15
  130.6 3.7 fusion.33
  134.4 2.6 fusion.36
  139.3 5.5 %collective-permute-done.1 = bf16[30,256]{1,0:T(8,128)(2,1)S(1)} collective-permute-done((bf16[30,256]{1,0:T(8,128)(2,1)S(1)}, bf16[30,256]{1,0:T(8,128)(2,1)S(1)}, u32[]{:S(2)}, u32[]{:S(2)}) %collective-permute-start.1) | collective-permute-done | bytes 15392 | tf_op jit(solution)/shard_map/ppermute | solution.py:21
  145.0 3.4 fusion.222
  149.1 4.3 %all-to-all-start = ((f32[8,1,768]{2,1,0:T(1,128)}), f32[8,1,768]{2,1,0:T(1,128)S(1)}, u32[]{:S(2)}, u32[]{:S(2)}) async-start(f32[8,1,768]{2,1,0:T(1,128)} %broadcast_in_dim.604), calls=%async_computation | async-start | bytes 49152 | tf_op jit(solution)/shard_map/all_to_all | solution.py:26
  153.3 5.4 %all-to-all-done = f32[8,1,768]{2,1,0:T(1,128)S(1)} async-done(((f32[8,1,768]{2,1,0:T(1,128)}), f32[8,1,768]{2,1,0:T(1,128)S(1)}, u32[]{:S(2)}, u32[]{:S(2)}) %all-to-all-start) | async-done | bytes 24608 | tf_op jit(solution)/shard_map/all_to_all | solution.py:26
  160.5 3.6 all-to-all-start.1
  164.1 29.7 %all-gather.11.cloned.1.call-done = bf16[3,2048,512]{2,1,0:T(8,128)(2,1)} async-done(((bf16[3,128,512]{2,1,0:T(8,128)(2,1)}), bf16[3,2048,512]{2,1,0:T(8,128)(2,1)}) %all-gather.11.cloned.1.call-update) | async-done | bytes 6291472 | tf_op jit(solution)/shard_map/all_gather | solution.py:63
  193.8 3.3 fusion.18
  197.3 27.5 %all-gather.15.cloned.1.call-done = bf16[3072,512]{1,0:T(8,128)(2,1)} async-done(((bf16[384,512]{1,0:T(8,128)(2,1)}), bf16[3072,512]{1,0:T(8,128)(2,1)}) %all-gather.15.cloned.1.call-update) | async-done | bytes 3145744 | tf_op jit(solution)/shard_map/all_gather | solution.py:67
  224.8 5.6 %copy.31 = f32[8,384,512]{1,2,0:T(8,128)} copy(bf16[8,384,512]{2,1,0:T(8,128)(2,1)} %bitcast.212) | data formatting | bytes 9437184 | tf_op jit(solution)/shard_map/convert_element_type | solution.py:68
  231.1 3.3 multiply_convert_fusion.1
  239.6 3.6 collective-permute-start.2
  243.3 4.1 %collective-permute-done.2 = bf16[30,256]{1,0:T(8,128)(2,1)S(1)} collective-permute-done((bf16[30,256]{1,0:T(8,128)(2,1)S(1)}, bf16[30,256]{1,0:T(8,128)(2,1)S(1)}, u32[]{:S(2)}, u32[]{:S(2)}) %collective-permute-start.2) | collective-permute-done | bytes 15392 | tf_op jit(solution)/shard_map/ppermute | solution.py:21
  247.5 3.4 fusion.221
  250.9 8.3 %all_to_all.33 = f32[8,1,768]{2,1,0:T(1,128)S(1)} all-to-all(f32[8,1,768]{2,1,0:T(1,128)S(1)} %broadcast_in_dim.606), channel_id=1, replica_groups=mesh['sp'=16,'tp'=8] {'tp'}, dimensions={0} | all-to-all | bytes 49152 | tf_op jit(solution)/shard_map/all_to_all | solution.py:26
  259.8 24.0 %all_to_all.34 = bf16[8,384,256]{1,2,0:T(8,128)(2,1)S(1)} all-to-all(bf16[8,384,256]{1,2,0:T(8,128)(2,1)S(1)} %broadcast_in_dim.607), channel_id=1, replica_groups=mesh['sp'=16,'tp'=8] {'tp'}, dimensions={0} | all-to-all | bytes 3145728 | tf_op jit(solution)/shard_map/all_to_all | solution.py:26
  283.8 3.4 fusion.17
  287.2 25.1 %all-gather.17.cloned.1.call-done = bf16[3072,512]{1,0:T(8,128)(2,1)} async-done(((bf16[384,512]{1,0:T(8,128)(2,1)}), bf16[3072,512]{1,0:T(8,128)(2,1)}) %all-gather.17.cloned.1.call-update) | async-done | bytes 3145744 | tf_op jit(solution)/shard_map/all_gather | solution.py:67
  312.3 5.6 %copy.34 = f32[8,384,512]{1,2,0:T(8,128)} copy(bf16[8,384,512]{2,1,0:T(8,128)(2,1)} %bitcast.214) | data formatting | bytes 9437184 | tf_op jit(solution)/shard_map/convert_element_type | solution.py:68
  318.6 3.3 multiply_convert_fusion
  327.2 3.4 collective-permute-start.3
  330.6 4.3 %collective-permute-done.3 = bf16[30,256]{1,0:T(8,128)(2,1)S(1)} collective-permute-done((bf16[30,256]{1,0:T(8,128)(2,1)S(1)}, bf16[30,256]{1,0:T(8,128)(2,1)S(1)}, u32[]{:S(2)}, u32[]{:S(2)}) %collective-permute-start.3) | collective-permute-done | bytes 15392 | tf_op jit(solution)/shard_map/ppermute | solution.py:21
  335.0 3.4 fusion.220
  338.5 8.3 %all_to_all.35 = f32[8,1,768]{2,1,0:T(1,128)S(1)} all-to-all(f32[8,1,768]{2,1,0:T(1,128)S(1)} %broadcast_in_dim.608), channel_id=1, replica_groups=mesh['sp'=16,'tp'=8] {'tp'}, dimensions={0} | all-to-all | bytes 49152 | tf_op jit(solution)/shard_map/all_to_all | solution.py:26
  347.3 24.0 %all_to_all.36 = bf16[8,384,256]{1,2,0:T(8,128)(2,1)S(1)} all-to-all(bf16[8,384,256]{1,2,0:T(8,128)(2,1)S(1)} %broadcast_in_dim.609), channel_id=1, replica_groups=mesh['sp'=16,'tp'=8] {'tp'}, dimensions={0} | all-to-all | bytes 3145728 | tf_op jit(solution)/shard_map/all_to_all | solution.py:26
  371.4 3.4 fusion.16
  (114 shorter events, 27.1 us)
Async XLA Ops:
  6.5 7.2 %copy-start.8 = (f32[3,4096]{1,0:T(4,128)S(1)}, f32[3,4096]{1,0:T(4,128)}, u32[]{:S(2)}) copy-start(f32[3,4096]{1,0:T(4,128)} %param.12) | copy-start | bytes 147460
  6.5 7.4 %copy-start.20 = (f32[3,256]{1,0:T(4,128)S(1)}, f32[3,256]{1,0:T(4,128)}, u32[]{:S(2)}) copy-start(f32[3,256]{1,0:T(4,128)} %param.16) | copy-start | bytes 9220
  6.5 8.0 %copy-start.21 = (f32[3,256]{1,0:T(4,128)S(1)}, f32[3,256]{1,0:T(4,128)}, u32[]{:S(2)}) copy-start(f32[3,256]{1,0:T(4,128)} %param.17) | copy-start | bytes 9220
  6.5 8.6 %copy-start.7 = (f32[3,31,256]{2,1,0:T(8,128)S(1)}, f32[3,31,256]{2,1,0:T(8,128)}, u32[]{:S(2)}) copy-start(f32[3,31,256]{2,1,0:T(8,128)} %param.15) | copy-start | bytes 285700
  6.5 32.2 %all-gather.13.cloned.1.call-start = ((), (), s32[]{:S(2)}) async-start(), calls=%async_computation.8 | async-start | bytes 3538944 | tf_op jit(solution)/shard_map/all_gather | solution.py:67
  7.3 123.3 %all-gather.9.cloned.1.call-start = ((), (), s32[]{:S(2)}) async-start(), calls=%async_computation.6 | async-start | bytes 13369344 | tf_op jit(solution)/shard_map/all_gather | solution.py:15
  9.5 184.3 %all-gather.11.cloned.1.call-start = ((), (), s32[]{:S(2)}) async-start(), calls=%async_computation.7 | async-start | bytes 6684672 | tf_op jit(solution)/shard_map/all_gather | solution.py:63
  10.3 7.6 %collective-permute-start = (s32[30]{0:T(128)S(1)}, s32[30]{0:T(128)S(1)}, u32[]{:S(2)}, u32[]{:S(2)}) collective-permute-start(s32[30]{0:T(128)S(1)} %slice.999), channel_id=1, source_target_pairs={{0,8},{8,16},{16,24},{24,32},{32,40},{40,48},{48,56},{56,64},{64,7... | collective-permute-start | bytes 368 | tf_op jit(solution)/shard_map/ppermute | solution.py:21
  130.6 3.7 copy-start.3
  134.3 10.6 %copy-start.10 = (f32[1,1,256]{2,1,0:T(1,128)S(1)}, f32[1,1,256]{2,1,0:T(1,128)}, u32[]{:S(2)}) copy-start(f32[1,1,256]{2,1,0:T(1,128)} %get-tuple-element.89) | copy-start | bytes 3076
  134.3 10.6 %copy-start.11 = (f32[1,1,256]{2,1,0:T(1,128)S(1)}, f32[1,1,256]{2,1,0:T(1,128)}, u32[]{:S(2)}) copy-start(f32[1,1,256]{2,1,0:T(1,128)} %get-tuple-element.90) | copy-start | bytes 3076
  134.3 10.6 %copy-start.12 = (f32[1,1,256]{2,1,0:T(1,128)S(1)}, f32[1,1,256]{2,1,0:T(1,128)}, u32[]{:S(2)}) copy-start(f32[1,1,256]{2,1,0:T(1,128)} %get-tuple-element.91) | copy-start | bytes 3076
  134.3 10.6 %copy-start.13 = (f32[1,1,256]{2,1,0:T(1,128)S(1)}, f32[1,1,256]{2,1,0:T(1,128)}, u32[]{:S(2)}) copy-start(f32[1,1,256]{2,1,0:T(1,128)} %get-tuple-element.92) | copy-start | bytes 3076
  134.4 10.6 %copy-start.19 = (f32[1,256]{1,0:T(1,128)S(1)}, f32[1,256]{1,0:T(1,128)}, u32[]{:S(2)}) copy-start(f32[1,256]{1,0:T(1,128)} %get-tuple-element.119) | copy-start | bytes 3076
  137.0 7.8 %collective-permute-start.1 = (bf16[30,256]{1,0:T(8,128)(2,1)S(1)}, bf16[30,256]{1,0:T(8,128)(2,1)S(1)}, u32[]{:S(2)}, u32[]{:S(2)}) collective-permute-start(bf16[30,256]{1,0:T(8,128)(2,1)S(1)} %slice.1247), channel_id=1, source_target_pairs={{0,8},{8,16},{16,24},{24,32},{32,40},{40,48},{48,56},{56,64},{64,7... | collective-permute-start | bytes 46088 | tf_op jit(solution)/shard_map/ppermute | solution.py:21
  145.0 8.4 %copy-start.22 = (f32[3,256]{1,0:T(4,128)S(1)}, f32[3,256]{1,0:T(4,128)}, u32[]{:S(2)}) copy-start(f32[3,256]{1,0:T(4,128)} %param.18) | copy-start | bytes 9220
  145.0 13.8 %copy-start.18 = (f32[1,256]{1,0:T(1,128)S(1)}, f32[1,256]{1,0:T(1,128)}, u32[]{:S(2)}) copy-start(f32[1,256]{1,0:T(1,128)} %get-tuple-element.113) | copy-start | bytes 3076
  148.4 45.4 %copy-start.4 = (bf16[384,512]{1,0:T(8,128)(2,1)S(1)}, bf16[384,512]{1,0:T(8,128)(2,1)}, u32[]{:S(2)}) copy-start(bf16[384,512]{1,0:T(8,128)(2,1)} %param.10) | copy-start | bytes 1179652
  149.1 9.7 %all-to-all-start = ((f32[8,1,768]{2,1,0:T(1,128)}), f32[8,1,768]{2,1,0:T(1,128)S(1)}, u32[]{:S(2)}, u32[]{:S(2)}) async-start(f32[8,1,768]{2,1,0:T(1,128)} %broadcast_in_dim.604), calls=%async_computation | async-start | bytes 49152 | tf_op jit(solution)/shard_map/all_to_all | solution.py:26
  160.5 33.3 %all-to-all-start.1 = ((bf16[8,384,256]{1,2,0:T(8,128)(2,1)}), bf16[8,384,256]{1,2,0:T(8,128)(2,1)S(1)}, u32[]{:S(2)}, u32[]{:S(2)}) async-start(bf16[8,384,256]{1,2,0:T(8,128)(2,1)} %broadcast_in_dim.605), calls=%async_computation.1 | async-start | bytes 3145728 | tf_op jit(solution)/shard_map/all_to_all | solution.py:26
  164.1 60.7 %all-gather.15.cloned.1.call-start = ((), (), s32[]{:S(2)}) async-start(), calls=%async_computation.9 | async-start | bytes 3538944 | tf_op jit(solution)/shard_map/all_gather | solution.py:67
  197.2 115.2 %all-gather.17.cloned.1.call-start = ((), (), s32[]{:S(2)}) async-start(), calls=%async_computation.10 | async-start | bytes 3538944 | tf_op jit(solution)/shard_map/all_gather | solution.py:67
  224.8 5.6 %copy-start.1 = (bf16[3072,512]{1,0:T(8,128)(2,1)S(1)}, bf16[3072,512]{1,0:T(8,128)(2,1)}, u32[]{:S(2)}) copy-start(bf16[3072,512]{1,0:T(8,128)(2,1)} %all-gather.15.cloned.1.call-done) | copy-start | bytes 9437188
  237.0 10.5 %copy-start.17 = (f32[1,256]{1,0:T(1,128)S(1)}, f32[1,256]{1,0:T(1,128)}, u32[]{:S(2)}) copy-start(f32[1,256]{1,0:T(1,128)} %get-tuple-element.120) | copy-start | bytes 3076
  239.6 7.7 %collective-permute-start.2 = (bf16[30,256]{1,0:T(8,128)(2,1)S(1)}, bf16[30,256]{1,0:T(8,128)(2,1)S(1)}, u32[]{:S(2)}, u32[]{:S(2)}) collective-permute-start(bf16[30,256]{1,0:T(8,128)(2,1)S(1)} %slice.1282), channel_id=1, source_target_pairs={{0,8},{8,16},{16,24},{24,32},{32,40},{40,48},{48,56},{56,64},{64,7... | collective-permute-start | bytes 46088 | tf_op jit(solution)/shard_map/ppermute | solution.py:21
  247.4 11.8 %copy-start.16 = (f32[1,256]{1,0:T(1,128)S(1)}, f32[1,256]{1,0:T(1,128)}, u32[]{:S(2)}) copy-start(f32[1,256]{1,0:T(1,128)} %get-tuple-element.114) | copy-start | bytes 3076
  250.9 32.9 %copy-start.6 = (bf16[384,512]{1,0:T(8,128)(2,1)S(1)}, bf16[384,512]{1,0:T(8,128)(2,1)}, u32[]{:S(2)}) copy-start(bf16[384,512]{1,0:T(8,128)(2,1)} %fusion.18) | copy-start | bytes 1179652
  312.3 5.6 %copy-start.2 = (bf16[3072,512]{1,0:T(8,128)(2,1)S(1)}, bf16[3072,512]{1,0:T(8,128)(2,1)}, u32[]{:S(2)}) copy-start(bf16[3072,512]{1,0:T(8,128)(2,1)} %all-gather.17.cloned.1.call-done) | copy-start | bytes 9437188
  324.5 10.5 %copy-start.15 = (f32[1,256]{1,0:T(1,128)S(1)}, f32[1,256]{1,0:T(1,128)}, u32[]{:S(2)}) copy-start(f32[1,256]{1,0:T(1,128)} %get-tuple-element.118) | copy-start | bytes 3076
  327.2 7.7 %collective-permute-start.3 = (bf16[30,256]{1,0:T(8,128)(2,1)S(1)}, bf16[30,256]{1,0:T(8,128)(2,1)S(1)}, u32[]{:S(2)}, u32[]{:S(2)}) collective-permute-start(bf16[30,256]{1,0:T(8,128)(2,1)S(1)} %slice.1317), channel_id=1, source_target_pairs={{0,8},{8,16},{16,24},{24,32},{32,40},{40,48},{48,56},{56,64},{64,7... | collective-permute-start | bytes 46088 | tf_op jit(solution)/shard_map/ppermute | solution.py:21
  335.0 11.8 %copy-start.14 = (f32[1,256]{1,0:T(1,128)S(1)}, f32[1,256]{1,0:T(1,128)}, u32[]{:S(2)}) copy-start(f32[1,256]{1,0:T(1,128)} %get-tuple-element.112) | copy-start | bytes 3076
  338.4 32.9 %copy-start.5 = (bf16[384,512]{1,0:T(8,128)(2,1)S(1)}, bf16[384,512]{1,0:T(8,128)(2,1)}, u32[]{:S(2)}) copy-start(bf16[384,512]{1,0:T(8,128)(2,1)} %fusion.17) | copy-start | bytes 1179652
  (2 other events, 6.5 us)
Sparse Core Ops, SparseCore 0:
  9.0 29.6 all-gather.12
  40.9 89.6 all-gather.8
  132.7 61.0 all-gather.10
  197.3 27.4 all-gather.14
  287.3 24.9 all-gather.16
